TPU v7x, 32 devices: a whole 2x2x4 slice. The times are simulated.
32 devices in a mesh: fs: 4 (over z), rep: 4 (over y, x), tp: 2 (over core).
Axes of the slice: x: 2, y: 2, z: 4, core: 2. Of those that a mesh axis runs over, the one named last changes fastest.
Arguments:
- saved_input: bfloat16 [16384, 2048], P(('fs', 'rep')), may hold values from -6 to 6
- cot_input: bfloat16 [16384, 1024], P(('fs', 'rep'), 'tp'), may hold values from -0.046875 to 0.046875
- cot_gate: bfloat16 [16384, 1024], P(('fs', 'rep'), 'tp'), may hold values from -0.046875 to 0.046875
- in_master: float32 [2048, 1024], P('fs', 'tp'), may hold values from -3 to 3
- gate_master: float32 [2048, 1024], P('fs', 'tp'), may hold values from -3 to 3
- in_factor: bfloat16 [2048, 256], P('fs'), may hold values from -0.125 to 0.125
- gate_factor: bfloat16 [2048, 256], P('fs'), may hold values from -0.125 to 0.125
- in_first: float32 [256, 1024], P('fs', 'tp'), may hold values from -6 to 6
- in_second: float32 [256, 1024], P('fs', 'tp'), may hold values from 0.5 to 2
- gate_first: float32 [256, 1024], P('fs', 'tp'), may hold values from -6 to 6
- gate_second: float32 [256, 1024], P('fs', 'tp'), may hold values from 0.5 to 2
Outputs:
- in_master_new: float32 [2048, 1024], P('fs', 'tp')
- gate_master_new: float32 [2048, 1024], P('fs', 'tp')
- in_update: float32 [2048, 1024], P('fs', 'tp')
- gate_update: float32 [2048, 1024], P('fs', 'tp')
- in_first_new: float32 [256, 1024], P('fs', 'tp')
- in_second_new: float32 [256, 1024], P('fs', 'tp')
- gate_first_new: float32 [256, 1024], P('fs', 'tp')
- gate_second_new: float32 [256, 1024], P('fs', 'tp')
- in_copy: bfloat16 [2048, 1024], P(None, 'tp')
- gate_copy: bfloat16 [2048, 1024], P(None, 'tp')
All inputs are finite; a program needn't handle non-finite values.
Results may differ from a plain program's by a relative error of at most 0.0065.
Values may be sent and summed in bfloat16 or wider, within the bound.
A program may use at most 64 MiB of HBM per device.

v0:
```python
import jax
import jax.numpy as jnp
from jax import lax
from jax.sharding import PartitionSpec as P

D = 2048
W = 1024


CONTRACT_ROWS = (((0,), (0,)), ((), ()))


def plain_rows(left, right):
    return lax.dot_general(left, right, CONTRACT_ROWS, preferred_element_type=jnp.float32)


def split_parts(values):
    upper = values.astype(jnp.bfloat16)
    lower = (values - upper.astype(jnp.float32)).astype(jnp.bfloat16)
    return (upper, lower)


def on_device(
    saved_input,
    cot_input,
    cot_gate,
    in_master,
    gate_master,
    in_factor,
    gate_factor,
    in_first,
    in_second,
    gate_first,
    gate_second,
):
    width = in_master.shape[1]
    in_basis = in_factor.astype(jnp.float32)
    gate_basis = gate_factor.astype(jnp.float32)
    in_whole, gate_whole = (
        lax.all_gather(in_factor, "fs", axis=0, tiled=True),
        lax.all_gather(gate_factor, "fs", axis=0, tiled=True),
    )
    in_upper, in_lower = split_parts(
        jnp.dot(saved_input, in_whole, preferred_element_type=jnp.float32)
    )
    gate_upper, gate_lower = split_parts(
        jnp.dot(saved_input, gate_whole, preferred_element_type=jnp.float32)
    )
    left = plain_rows(in_upper, cot_input)
    left = left + plain_rows(in_lower, cot_input)
    right = plain_rows(gate_upper, cot_gate)
    right = right + plain_rows(gate_lower, cot_gate)
    partial_low = lax.psum_scatter(
        jnp.concatenate([left, right], axis=1).astype(jnp.bfloat16),
        "fs",
        scatter_dimension=0,
        tiled=True,
    )
    low = lax.psum(partial_low, "rep").astype(jnp.float32)
    first_old = jnp.concatenate([in_first, gate_first], axis=1)
    second_old = jnp.concatenate([in_second, gate_second], axis=1)
    first_new = 0.8 * first_old + 0.2 * low
    second_new = 0.95 * second_old + 0.05 * low * low
    normed = first_new / jnp.sqrt(second_new)
    piece = lax.all_gather(normed, "fs", axis=0, tiled=True)
    left = jnp.dot(in_basis, piece[:, :width], precision=lax.Precision.HIGHEST)
    right = jnp.dot(gate_basis, piece[:, width:], precision=lax.Precision.HIGHEST)
    in_square, gate_square = lax.psum((jnp.sum(left * left), jnp.sum(right * right)), ("fs", "tp"))
    in_update = left / jnp.sqrt(in_square / (D * W) + 0.1)
    gate_update = right / jnp.sqrt(gate_square / (D * W) + 0.1)
    in_master_new = in_master - 0.05 * in_update
    gate_master_new = gate_master - 0.05 * gate_update
    in_copy, gate_copy = (
        lax.all_gather(in_master_new.astype(jnp.bfloat16), "fs", axis=0, tiled=True),
        lax.all_gather(gate_master_new.astype(jnp.bfloat16), "fs", axis=0, tiled=True),
    )
    return (
        in_master_new,
        gate_master_new,
        in_update,
        gate_update,
        first_new[:, :width],
        second_new[:, :width],
        first_new[:, width:],
        second_new[:, width:],
        in_copy,
        gate_copy,
    )


def solution(mesh):
    placed = (
        P(("fs", "rep"), None),
        P(("fs", "rep"), "tp"),
        P(("fs", "rep"), "tp"),
        P("fs", "tp"),
        P("fs", "tp"),
        P("fs", None),
        P("fs", None),
        P("fs", "tp"),
        P("fs", "tp"),
        P("fs", "tp"),
        P("fs", "tp"),
    )
    return jax.shard_map(
        on_device,
        mesh=mesh,
        in_specs=placed,
        out_specs=(
            P("fs", "tp"),
            P("fs", "tp"),
            P("fs", "tp"),
            P("fs", "tp"),
            P("fs", "tp"),
            P("fs", "tp"),
            P("fs", "tp"),
            P("fs", "tp"),
            P(None, "tp"),
            P(None, "tp"),
        ),
        check_vma=False,
    )
```

profile of v0, /device:TPU:0, one launch (start us, length us, event | category | flops | bytes accessed | tf_op | source)
XLA Modules:
  0.0 296.7 jit_solution(4529653988439130760)
XLA Ops:
  7.2 0.0 copy-start
  7.2 0.0 all-gather.8.cloned.1.call-start
  7.2 0.7 all-gather.8.cloned.1.call-update
  7.9 0.0 all-gather.6.cloned.1.call-start
  8.0 0.7 all-gather.6.cloned.1.call-update
  8.7 0.0 reduce-scatter.2.cloned.1.call-start
  8.7 31.6 %all-gather.8.cloned.1.call-done = bf16[2048,256]{1,0:T(8,128)(2,1)} async-done(((bf16[512,256]{1,0:T(8,128)(2,1)}), bf16[2048,256]{1,0:T(8,128)(2,1)}) %all-gather.8.cloned.1.call-update) | async-done | bytes 1048592 | tf_op jit(solution)/shard_map/all_gather | solution.py:41
  40.3 3.7 %fusion.21 = f32[1024,256]{1,0:T(8,128)S(1)} fusion(bf16[1024,2048]{1,0:T(8,128)(2,1)} %param.11, bf16[2048,256]{1,0:T(8,128)(2,1)} %all-gather.8.cloned.1.call-done), kind=kOutput, calls=%fused_computation.35 | convolution fusion | flops 1073741824 | bytes 6291456 | tf_op jit(solution)/shard_map/dot_general | solution.py:47
  44.1 0.5 fusion.9
  44.6 1.2 fusion.1
  45.8 23.5 %all-gather.6.cloned.1.call-done = bf16[2048,256]{1,0:T(8,128)(2,1)} async-done(((bf16[512,256]{1,0:T(8,128)(2,1)}), bf16[2048,256]{1,0:T(8,128)(2,1)}) %all-gather.6.cloned.1.call-update) | async-done | bytes 1048592 | tf_op jit(solution)/shard_map/all_gather | solution.py:40
  69.3 3.7 %fusion.20 = f32[1024,256]{1,0:T(8,128)S(1)} fusion(bf16[1024,2048]{1,0:T(8,128)(2,1)} %param.11, bf16[2048,256]{1,0:T(8,128)(2,1)} %all-gather.6.cloned.1.call-done), kind=kOutput, calls=%fused_computation.34 | convolution fusion | flops 1073741824 | bytes 6291456 | tf_op jit(solution)/shard_map/dot_general | solution.py:44
  73.0 0.0 copy-start.6
  73.0 0.0 copy-start.7
  73.0 0.0 copy-start.2
  73.1 0.5 fusion.12
  73.6 0.5 fusion
  74.1 0.0 copy-start.4
  74.1 0.9 pad_maximum_fusion
  74.9 0.0 reduce-scatter.2.cloned.1.call-update
  75.0 0.0 all-reduce.3.cloned.1.call-start
  75.0 21.3 %reduce-scatter.2.cloned.1.call-done = bf16[64,1024]{1,0:T(8,128)(2,1)} async-done(((bf16[256,1024]{1,0:T(8,128)(2,1)}), bf16[64,1024]{1,0:T(8,128)(2,1)}) %reduce-scatter.2.cloned.1.call-update) | async-done | bytes 131088 | tf_op jit(solution)/shard_map/reduce_scatter | solution.py:53
  96.3 0.0 all-reduce.3.cloned.1.call-update
  96.3 0.0 all-gather.10.cloned.1.call-start
  96.4 43.2 %all-reduce.3.cloned.1.call-done = bf16[64,1024]{1,0:T(8,128)(2,1)} async-done(((bf16[64,1024]{1,0:T(8,128)(2,1)}), bf16[64,1024]{1,0:T(8,128)(2,1)}) %all-reduce.3.cloned.1.call-update) | async-done | bytes 131088 | tf_op jit(solution)/shard_map/psum | solution.py:59
  139.6 2.0 rsqrt_multiply_fusion
  141.6 0.0 all-gather.10.cloned.1.call-update
  141.6 0.0 all-gather.12.cloned.1.call-start
  141.7 1.3 copy.21
  143.0 26.8 %all-gather.10.cloned.1.call-done = f32[256,1024]{1,0:T(8,128)} async-done(((f32[64,1024]{1,0:T(8,128)}), f32[256,1024]{1,0:T(8,128)}) %all-gather.10.cloned.1.call-update) | async-done | bytes 1048592 | tf_op jit(solution)/shard_map/all_gather | solution.py:65
  169.8 3.6 %multiply_reduce_fusion = (f32[]{:T(128)}, f32[512,512]{1,0:T(8,128)}) fusion(bf16[512,256]{1,0:T(8,128)(2,1)S(1)} %copy-done.3, f32[256,1024]{1,0:T(8,128)} %all-gather.10.cloned.1.call-done), kind=kOutput, calls=%fused_computation.6 | convolution fusion | flops 805830656 | bytes 1835012 | tf_op jit(solution)/shard_map/dot_general | solution.py:67
  173.4 3.6 %multiply_reduce_fusion.1 = (f32[]{:T(128)}, f32[512,512]{1,0:T(8,128)}) fusion(bf16[512,256]{1,0:T(8,128)(2,1)S(1)} %copy-done.4, f32[256,1024]{1,0:T(8,128)} %all-gather.10.cloned.1.call-done), kind=kOutput, calls=%fused_computation.9 | convolution fusion | flops 805830656 | bytes 1835012 | tf_op jit(solution)/shard_map/dot_general | solution.py:66
  177.0 15.3 %all-reduce = (f32[]{:T(128)}, f32[]{:T(128)}) all-reduce(f32[]{:T(128)} %get-tuple-element.35, f32[]{:T(128)} %get-tuple-element.37), channel_id=1, replica_groups=mesh['fs'=4,'rep'=4,'tp'=2] {'fs','tp'}, use_global_device_ids=true, to_apply=%region_3.0 | all-reduce | flops 2 | bytes 16 | tf_op jit(solution)/shard_map/psum | solution.py:68
  193.0 2.7 fusion.15
  195.7 0.0 all-gather.12.cloned.1.call-update
  195.7 0.0 all-gather.14.cloned.1.call-start
  195.7 2.5 copy.22
  199.0 3.4 %fusion.14 = (bf16[512,512]{0,1:T(8,128)(2,1)}, f32[512,512]{0,1:T(8,128)}, f32[512,512]{0,1:T(8,128)}) fusion(f32[512,512]{0,1:T(8,128)} %copy.22, f32[512,512]{1,0:T(8,128)} %get-tuple-element.38, f32[]{:T(128)S(6)} %sqrt.11), kind=kLoop, calls=%fused_computation.30 | loop fusion | flops 1048576 | bytes 4718596 | tf_op jit(solution)/shard_map/convert_element_type | solution.py:75
  202.4 0.0 all-gather.14.cloned.1.call-update
  202.4 1.8 fusion.18
  204.2 2.5 copy.24
  206.7 2.5 copy.26
  209.3 1.3 copy.23
  210.6 1.3 copy.25
  211.9 28.0 %all-gather.12.cloned.1.call-done = bf16[2048,512]{0,1:T(8,128)(2,1)} async-done(((bf16[512,512]{0,1:T(8,128)(2,1)}), bf16[2048,512]{0,1:T(8,128)(2,1)}) %all-gather.12.cloned.1.call-update) | async-done | bytes 2097168 | tf_op jit(solution)/shard_map/all_gather | solution.py:74
  239.9 3.9 %copy.27 = bf16[2048,512]{1,0:T(8,128)(2,1)} copy(bf16[2048,512]{0,1:T(8,128)(2,1)} %all-gather.12.cloned.1.call-done) | data formatting | bytes 4194304
  243.8 42.1 %all-gather.14.cloned.1.call-done = bf16[2048,512]{0,1:T(8,128)(2,1)} async-done(((bf16[512,512]{0,1:T(8,128)(2,1)}), bf16[2048,512]{0,1:T(8,128)(2,1)}) %all-gather.14.cloned.1.call-update) | async-done | bytes 2097168 | tf_op jit(solution)/shard_map/all_gather | solution.py:75
  285.9 3.9 %copy.28 = bf16[2048,512]{1,0:T(8,128)(2,1)} copy(bf16[2048,512]{0,1:T(8,128)(2,1)} %all-gather.14.cloned.1.call-done) | data formatting | bytes 4194304
  (11 shorter events, 0.0 us)
Async XLA Ops:
  7.2 36.9 %copy-start = (bf16[1024,512]{1,0:T(8,128)(2,1)S(1)}, bf16[1024,512]{1,0:T(8,128)(2,1)}, u32[]{:S(2)}) copy-start(bf16[1024,512]{1,0:T(8,128)(2,1)} %param.13) | copy-start | bytes 3145732
  7.2 33.1 %all-gather.8.cloned.1.call-start = ((), (), s32[]{:S(2)}) async-start(), calls=%async_computation.2 | async-start | bytes 1310720 | tf_op jit(solution)/shard_map/all_gather | solution.py:41
  7.9 61.3 %all-gather.6.cloned.1.call-start = ((), (), s32[]{:S(2)}) async-start(), calls=%async_computation.1 | async-start | bytes 1310720 | tf_op jit(solution)/shard_map/all_gather | solution.py:40
  8.7 87.6 %reduce-scatter.2.cloned.1.call-start = ((), (), s32[]{:S(2)}) async-start(), calls=%async_computation.3 | async-start | bytes 655360 | tf_op jit(solution)/shard_map/reduce_scatter | solution.py:53
  45.8 27.3 %copy-start.1 = (bf16[1024,512]{1,0:T(8,128)(2,1)S(1)}, bf16[1024,512]{1,0:T(8,128)(2,1)}, u32[]{:S(2)}) copy-start(bf16[1024,512]{1,0:T(8,128)(2,1)} %param.12) | copy-start | bytes 3145732
  73.0 1.0 copy-start.6
  73.0 66.5 %copy-start.7 = (f32[64,512]{1,0:T(8,128)S(1)}, f32[64,512]{1,0:T(8,128)}, u32[]{:S(2)}) copy-start(f32[64,512]{1,0:T(8,128)} %param.21) | copy-start | bytes 393220
  73.0 68.6 %copy-start.2 = (f32[512,512]{1,0:T(8,128)S(1)}, f32[512,512]{1,0:T(8,128)}, u32[]{:S(2)}) copy-start(f32[512,512]{1,0:T(8,128)} %param.14) | copy-start | bytes 3145732
  73.5 96.2 %copy-start.3 = (bf16[512,256]{1,0:T(8,128)(2,1)S(1)}, bf16[512,256]{1,0:T(8,128)(2,1)}, u32[]{:S(2)}) copy-start(bf16[512,256]{1,0:T(8,128)(2,1)} %param.17) | copy-start | bytes 786436
  74.1 99.3 %copy-start.4 = (bf16[512,256]{1,0:T(8,128)(2,1)S(1)}, bf16[512,256]{1,0:T(8,128)(2,1)}, u32[]{:S(2)}) copy-start(bf16[512,256]{1,0:T(8,128)(2,1)} %param.16) | copy-start | bytes 786436
  75.0 64.6 %all-reduce.3.cloned.1.call-start = ((), (), s32[]{:S(2)}) async-start(), calls=%async_computation.4 | async-start | bytes 262144 | tf_op jit(solution)/shard_map/psum | solution.py:59
  96.3 73.4 %all-gather.10.cloned.1.call-start = ((), (), s32[]{:S(2)}) async-start(), calls=%async_computation.5 | async-start | bytes 1310720 | tf_op jit(solution)/shard_map/all_gather | solution.py:65
  141.6 98.2 %all-gather.12.cloned.1.call-start = ((), (), s32[]{:S(2)}) async-start(), calls=%async_computation.6 | async-start | bytes 2621440 | tf_op jit(solution)/shard_map/all_gather | solution.py:74
  195.7 6.7 %copy-start.5 = (f32[64,1024]{1,0:T(8,128)S(1)}, f32[64,1024]{1,0:T(8,128)}, u32[]{:S(2)}) copy-start(f32[64,1024]{1,0:T(8,128)} %get-tuple-element.29) | copy-start | bytes 786436
  195.7 90.2 %all-gather.14.cloned.1.call-start = ((), (), s32[]{:S(2)}) async-start(), calls=%async_computation.7 | async-start | bytes 2621440 | tf_op jit(solution)/shard_map/all_gather | solution.py:75
Sparse Core Ops, SparseCore 0:
  9.6 30.6 all-gather.7
  41.9 27.3 all-gather.5
  75.1 21.1 reduce-scatter.1
  99.1 40.4 all-reduce.2
  141.7 27.9 all-gather.9
  195.8 44.0 all-gather.11
  241.4 44.4 all-gather.13
where the time goes:
time: 297 us
  waiting for transfers between devices  218 us (73%)
  local copies, waits for them, and re-layouts  21.2 us (7%)
  matrix products  17.3 us (6%)
  between operations  15.7 us (5%)
  blocking collectives  15.3 us (5%)
  other arithmetic  8.96 us (3%)
    psum x1, waiting for transfers between devices, on_device(): low = lax.psum(partial_low, 'rep').astype(jnp.float32)  43.2 us
    all_gather x1, waiting for transfers between devices, on_device(): lax.all_gather(gate_master_new.astype(jnp.bfloat16), 'fs', axis=0, tiled=...  42.1 us
    all_gather x1, waiting for transfers between devices, on_device(): lax.all_gather(gate_factor, 'fs', axis=0, tiled=True)  31.6 us
    all_gather x1, waiting for transfers between devices, on_device(): lax.all_gather(in_master_new.astype(jnp.bfloat16), 'fs', axis=0, tiled=True)  28 us
    all_gather x1, waiting for transfers between devices, on_device(): piece = lax.all_gather(normed, 'fs', axis=0, tiled=True)  26.8 us
    all_gather x1, waiting for transfers between devices, on_device(): lax.all_gather(in_factor, 'fs', axis=0, tiled=True)  23.5 us
    reduce_scatter x1, waiting for transfers between devices, on_device(): lax.psum_scatter(jnp.concatenate([left, right], axis=1).astype(jnp.bfloat...  21.3 us
    unnamed x24, local copies, waits for them, and re-layouts  19.4 us
  transfers between devices with their start and end apart: 7, of which 7 were waited for; matrix products, arithmetic and copies ran while one was open for 9% of the time, Pallas kernels for 0%

commit v1 on v0

v1 whole, which is shorter than its diff:
```python
import functools

import jax
import jax.numpy as jnp
from jax import lax
from jax.experimental import pallas as pl
from jax.experimental.pallas import tpu as pltpu
from jax.sharding import PartitionSpec as P

MESH = pl.DeviceIdType.MESH
BF = jnp.bfloat16
F32 = jnp.float32
LIMIT = 60 * 1024 * 1024


def exchange_kernel(
    n_f, n_r,
    x_hbm, ci_hbm, cg_hbm, mi_hbm, mg_hbm, fi_hbm, fg_hbm, p0_hbm, s0_hbm, p1_hbm, s1_hbm,
    masters_out, factor_out, normed_out, low_out, square_out,
    x_v, cot_v, fac, mas32, mas16, old, acc, pbuf, r1buf, sumbuf, r2buf, nall, lall, sq,
    loc, f1s, f1r, f2s, f2r, f3s, f3r, m1s, m1r, m2s, m2r, r1s, r1r, r2s, r2r,
    a1s, a1r, als, alr, a2s, a2r, sqs, sqr,
):
    f, r, t = lax.axis_index("fs"), lax.axis_index("rep"), lax.axis_index("tp")
    tokens = x_v.shape[0]
    rows = mi_hbm.shape[0]
    width = mi_hbm.shape[1]
    rank = fi_hbm.shape[1]
    own = p0_hbm.shape[0]
    cw = width // n_r
    half = rows // 2
    piece = half // n_r
    quarter = rows // n_r
    ks = sorted(range(1, n_f), key=lambda k: min(k, n_f - k))
    js = list(range(1, n_r))

    def f_to(k):
        return lax.rem(f + k, n_f)

    def f_from(k):
        return lax.rem(f - k + n_f, n_f)

    def r_to(j):
        return lax.rem(r + j, n_r)

    def span(start, size, unit):
        return pl.ds(pl.multiple_of(start, unit), size)

    sent = []

    def send(src, dst, ss, rs, ff, rr, tt):
        c = pltpu.make_async_remote_copy(
            src_ref=src, dst_ref=dst, send_sem=ss, recv_sem=rs,
            device_id=(ff, rr, tt), device_id_type=MESH)
        c.start()
        sent.append(c)
        return c

    def local(src, dst, i):
        c = pltpu.make_async_copy(src, dst, loc.at[i])
        c.start()
        return c

    mine = span(f * rows, rows, rows)
    lf = [local(fi_hbm, fac.at[mine, pl.ds(0, rank)], 0), local(fg_hbm, fac.at[mine, pl.ds(rank, rank)], 1)]
    lm = [local(mi_hbm, mas32.at[0], 2), local(mg_hbm, mas32.at[1], 3)]
    lx = local(x_hbm, x_v, 4)
    lc = [local(ci_hbm, cot_v.at[0], 5), local(cg_hbm, cot_v.at[1], 6)]
    lo = [local(h, old.at[i], 7 + i) for i, h in enumerate((p0_hbm, s0_hbm, p1_hbm, s1_hbm))]

    barrier = pltpu.get_barrier_semaphore()
    for k in ks:
        pl.semaphore_signal(barrier, inc=1, device_id=(f_to(k), r, t), device_id_type=MESH)
    for j in js:
        pl.semaphore_signal(barrier, inc=1, device_id=(f, r_to(j), t), device_id_type=MESH)
    pl.semaphore_signal(barrier, inc=1, device_id=(f, r, 1 - t), device_id_type=MESH)
    pl.semaphore_wait(barrier, len(ks) + len(js) + 1)

    for c in lf:
        c.wait()
    f1 = {}
    for k in ks:
        at = span(f * rows + t * half + r * piece, piece, piece)
        f1[k] = send(fac.at[at], fac.at[at], f1s.at[k], f1r.at[k], f_to(k), r, t)
    for c in lm:
        c.wait()
    for g in range(2):
        mas16[:, g * width:(g + 1) * width] = mas32[g].astype(BF)
    m1 = {}
    for k in ks:
        m1[k] = send(
            mas16.at[span(r * quarter, quarter, quarter)],
            masters_out.at[span(f * rows + r * quarter, quarter, quarter)],
            m1s.at[k], m1r.at[k], f_to(k), r, t)
    lown = local(mas16, masters_out.at[mine], 11)
    lx.wait()

    tile = min(256, tokens)

    blocked = rows % 128 == 0

    def project(source, first):
        if not blocked and not first:
            return
        depth = span(source * rows, rows, rows) if blocked else slice(None)
        weights = fac[depth, :]

        def step(i, carry):
            at = span(i * tile, tile, tile)
            part = jnp.dot(x_v[at, depth], weights, preferred_element_type=F32)
            acc[at, :] = part if first else acc[at, :] + part
            return carry

        lax.fori_loop(0, tokens // tile, step, 0)

    f2 = {}

    def spread(k):
        f1[k].wait_recv()
        at = span(f_from(k) * rows + t * half + r * piece, piece, piece)
        for j in js:
            f2[k, j] = send(fac.at[at], fac.at[at], f2s.at[k, j], f2r.at[k, j], f, r_to(j), t)

    if blocked:
        project(f, True)
    for k in ks:
        spread(k)
    f3 = {}
    for k in ks:
        for j in js:
            f2[k, j].wait_recv()
        at = span(f_from(k) * rows + t * half, half, half)
        f3[k] = send(fac.at[at], fac.at[at], f3s.at[k], f3r.at[k], f, r, 1 - t)
    for k in ks:
        f3[k].wait_recv()
        project(f_from(k), False)
    if not blocked:
        project(f, True)
    lfac = local(fac, factor_out, 12)

    for c in lc:
        c.wait()
    r1 = {}
    for g in range(2):
        turned = acc[:, g * rank:(g + 1) * rank].astype(BF).T
        part = jnp.dot(turned, cot_v[g], preferred_element_type=F32).astype(BF)
        for q in range(n_r):
            pbuf[q, g] = part[:, q * cw:(q + 1) * cw]
        for j in js:
            r1[j, g] = send(pbuf.at[r_to(j), g], r1buf.at[j, g], r1s.at[j, g], r1r.at[j, g], f, r_to(j), t)

    m2 = {}

    def spread_masters(k):
        m1[k].wait_recv()
        at = span(f_from(k) * rows + r * quarter, quarter, quarter)
        for j in js:
            m2[k, j] = send(masters_out.at[at], masters_out.at[at], m2s.at[k, j], m2r.at[k, j], f, r_to(j), t)

    cut1 = (len(ks) + 2) // 3
    cut2 = (2 * len(ks) + 2) // 3
    for k in ks[:cut1]:
        spread_masters(k)

    for g in range(2):
        total = pbuf[r, g].astype(F32)
        for j in js:
            r1[j, g].wait_recv()
            total = total + r1buf[j, g].astype(F32)
        sumbuf[g] = total.astype(BF)
    r2 = {}
    for k in ks:
        r2[k] = send(
            sumbuf.at[:, span(f_to(k) * own, own, own), :], r2buf.at[k],
            r2s.at[k], r2r.at[k], f_to(k), r, t)
    low = sumbuf[:, span(f * own, own, own), :].astype(F32)
    for k in ks:
        r2[k].wait_recv()
        low = low + r2buf[k].astype(F32)
    for c in lo:
        c.wait()
    lall[r] = low.astype(BF)
    columns = span(r * cw, cw, cw)
    for g in range(2):
        first = 0.8 * old[2 * g, :, columns] + 0.2 * low[g]
        second = 0.95 * old[2 * g + 1, :, columns] + 0.05 * low[g] * low[g]
        nall[r, g, span(f * own, own, own), :] = (first / jnp.sqrt(second)).astype(BF)
    a1 = {}
    for k in ks:
        at = nall.at[r, :, span(f * own, own, own), :]
        a1[k] = send(at, at, a1s.at[k], a1r.at[k], f_to(k), r, t)
    al = {}
    for j in js:
        al[j] = send(lall.at[r], lall.at[r], als.at[j], alr.at[j], f, r_to(j), t)
    for k in ks[cut1:cut2]:
        spread_masters(k)
    for k in ks:
        a1[k].wait_recv()
    a2 = {}
    for j in js:
        a2[j] = send(nall.at[r], nall.at[r], a2s.at[j], a2r.at[j], f, r_to(j), t)
    for k in ks[cut2:]:
        spread_masters(k)
    for j in js:
        al[j].wait_recv()
    llow = local(lall, low_out, 13)
    for j in js:
        a2[j].wait_recv()
    lnorm = local(nall, normed_out, 14)

    for g in range(2):
        whole = jnp.concatenate([nall[q, g] for q in range(n_r)], axis=1)

        def square(i, total):
            at = span(i * 256, 256, 256)
            full = jnp.dot(fac[at, g * rank:(g + 1) * rank], whole, preferred_element_type=F32)
            return total + jnp.sum((full * full).reshape(32, 8, width), axis=0)

        total = lax.fori_loop(0, fac.shape[0] // 256, square, jnp.zeros((8, width), F32))
        part = total[:, :128]
        for q in range(1, width // 128):
            part = part + total[:, q * 128:(q + 1) * 128]
        sq[t, g] = part
    other = send(sq.at[t], sq.at[t], sqs, sqr, f, r, 1 - t)
    other.wait_recv()
    lsq = local(sq, square_out, 15)
    for c in (lown, lfac, llow, lnorm, lsq):
        c.wait()
    for k in ks:
        for j in js:
            m2[k, j].wait_recv()
    for c in sent:
        c.wait_send()


def finish_kernel(
    entries,
    fac, mas, nor, low, sqr, fi, fg, mi, mg, p0, s0, p1, s1,
    mi_new, mg_new, ui, ug, p0n, s0n, p1n, s1n, ci, cg,
):
    n_r = nor.shape[0]
    width = mi.shape[1]
    rank = fi.shape[1]
    new = ((p0, s0, p0n, s0n), (p1, s1, p1n, s1n))

    @pl.when(pl.program_id(0) == 0)
    def _():
        for g, (p, s, pn, sn) in enumerate(new):
            got = jnp.concatenate([low[q, g] for q in range(n_r)], axis=1).astype(F32)
            pn[...] = 0.8 * p[...] + 0.2 * got
            sn[...] = 0.95 * s[...] + 0.05 * got * got

    for g, (own_f, own_m, m_new, up, copy) in enumerate(((fi, mi, mi_new, ui, ci), (fg, mg, mg_new, ug, cg))):
        whole = jnp.concatenate([nor[q, g] for q in range(n_r)], axis=1)
        square = jnp.sum(sqr[0, g] + sqr[1, g], keepdims=True)
        scale = 1.0 / jnp.sqrt(square / entries + 0.1)
        full = jnp.dot(own_f[...], whole, preferred_element_type=F32)
        update = full * scale
        up[...] = update
        m_new[...] = own_m[...] - 0.05 * update
        rest = jnp.dot(fac[:, g * rank:(g + 1) * rank], whole, preferred_element_type=F32)
        base = mas[:, g * width:(g + 1) * width].astype(F32)
        copy[...] = (base - 0.05 * (rest * scale)).astype(BF)


def on_device(n_f, n_r, n_t, x, ci, cg, mi, mg, fi, fg, p0, s0, p1, s1):
    tokens, d = x.shape
    rows, width = mi.shape
    rank = fi.shape[1]
    own = p0.shape[0]
    cw = width // n_r
    any_ = pl.BlockSpec(memory_space=pl.ANY)
    dma = pltpu.SemaphoreType.DMA
    S = jax.ShapeDtypeStruct
    masters, factors, normed, low, squares = pl.pallas_call(
        functools.partial(exchange_kernel, n_f, n_r),
        out_shape=(
            S((d, 2 * width), BF),
            S((d, 2 * rank), BF),
            S((n_r, 2, rank, cw), BF),
            S((n_r, 2, own, cw), BF),
            S((2, 2, 8, 128), F32),
        ),
        in_specs=[any_] * 11,
        out_specs=(any_,) * 5,
        scratch_shapes=[
            pltpu.VMEM((tokens, d), BF),
            pltpu.VMEM((2, tokens, width), BF),
            pltpu.VMEM((d, 2 * rank), BF),
            pltpu.VMEM((2, rows, width), F32),
            pltpu.VMEM((rows, 2 * width), BF),
            pltpu.VMEM((4, own, width), F32),
            pltpu.VMEM((tokens, 2 * rank), F32),
            pltpu.VMEM((n_r, 2, rank, cw), BF),
            pltpu.VMEM((n_r, 2, rank, cw), BF),
            pltpu.VMEM((2, rank, cw), BF),
            pltpu.VMEM((n_f, 2, own, cw), BF),
            pltpu.VMEM((n_r, 2, rank, cw), BF),
            pltpu.VMEM((n_r, 2, own, cw), BF),
            pltpu.VMEM((2, 2, 8, 128), F32),
            dma((16,)),
            dma((n_f,)), dma((n_f,)),
            dma((n_f, n_r)), dma((n_f, n_r)),
            dma((n_f,)), dma((n_f,)),
            dma((n_f,)), dma((n_f,)),
            dma((n_f, n_r)), dma((n_f, n_r)),
            dma((n_r, 2)), dma((n_r, 2)),
            dma((n_f,)), dma((n_f,)),
            dma((n_f,)), dma((n_f,)),
            dma((n_r,)), dma((n_r,)),
            dma((n_r,)), dma((n_r,)),
            dma, dma,
        ],
        compiler_params=pltpu.CompilerParams(
            collective_id=0, has_side_effects=True, vmem_limit_bytes=LIMIT),
        name="exchange",
    )(x, ci, cg, mi, mg, fi, fg, p0, s0, p1, s1)

    steps = 8
    dt, rt = d // steps, rows // steps

    def tiled(a, b):
        return pl.BlockSpec((a, b), lambda i: (i, 0))

    def fixed(shape):
        return pl.BlockSpec(shape, lambda i: (0,) * len(shape))

    moment = fixed((own, width))
    return pl.pallas_call(
        functools.partial(finish_kernel, d * width * n_t),
        grid=(steps,),
        out_shape=(S((rows, width), F32),) * 4 + (S((own, width), F32),) * 4 + (S((d, width), BF),) * 2,
        in_specs=[
            tiled(dt, 2 * rank), tiled(dt, 2 * width),
            fixed(normed.shape), fixed(low.shape), fixed(squares.shape),
            tiled(rt, rank), tiled(rt, rank), tiled(rt, width), tiled(rt, width),
            moment, moment, moment, moment,
        ],
        out_specs=(tiled(rt, width),) * 4 + (moment,) * 4 + (tiled(dt, width),) * 2,
        compiler_params=pltpu.CompilerParams(
            dimension_semantics=("arbitrary",), vmem_limit_bytes=LIMIT // 2),
        name="finish",
    )(factors, masters, normed, low, squares, fi, fg, mi, mg, p0, s0, p1, s1)


def solution(mesh):
    tokens = P(("fs", "rep"), None)
    cots = P(("fs", "rep"), "tp")
    both, tall, wide = P("fs", "tp"), P("fs", None), P(None, "tp")
    return jax.shard_map(
        functools.partial(on_device, mesh.shape["fs"], mesh.shape["rep"], mesh.shape["tp"]),
        mesh=mesh,
        in_specs=(tokens, cots, cots, both, both, tall, tall, both, both, both, both),
        out_specs=(both,) * 8 + (wide,) * 2,
        check_vma=False,
    )
```

time: 297 us -> 89.8 us (0.30)
  waiting for transfers between devices: 218 us -> 0 us
  Pallas kernels: 0 us -> 82.2 us
  matrix products: 17.3 us -> 0 us
  blocking collectives: 15.3 us -> 0 us
  between operations: 15.7 us -> 0.79 us
  local copies, waits for them, and re-layouts: 21.2 us -> 6.47 us
  other arithmetic: 8.96 us -> 0 us
    all_gather x5 -> x0, waiting for transfers between devices: 152 us -> none  [the longest x1 42.1 us: on_device(): lax.all_gather(gate_master_new.astype(jnp.bfloat16), 'fs', axis=0, tiled=...]
    pallas_call x0 -> x2, Pallas kernels: none -> 82.2 us  [the longest x1 76.4 us: on_device(): pl.pallas_call(functools.partial(exchange_kernel, n_f, n_r), out_shape=(S...]
    psum x1 -> x0, waiting for transfers between devices: 43.2 us -> none  [on_device(): low = lax.psum(partial_low, 'rep').astype(jnp.float32)]
    reduce_scatter x1 -> x0, waiting for transfers between devices: 21.3 us -> none  [on_device(): lax.psum_scatter(jnp.concatenate([left, right], axis=1).astype(jnp.bfloat...]
    dot_general x8 -> x0, matrix products: 17.3 us -> none  [the longest x1 3.74 us: on_device(): jnp.dot(saved_input, gate_whole, preferred_element_type=jnp.float32)]
    psum x1 -> x0, blocking collectives: 15.3 us -> none  [on_device(): lax.psum((jnp.sum(left * left), jnp.sum(right * right)), ('fs', 'tp'))]
    unnamed x24 -> x26, local copies, waits for them, and re-layouts: 19.4 us -> 6.47 us
    convert_element_type x2 -> x0, other arithmetic: 6.08 us -> none  [the longest x1 3.41 us: on_device(): gate_master_new.astype(jnp.bfloat16)]
  transfers between devices with their start and end apart: 7 -> 0, of which waited for: 7 -> 0; matrix products, arithmetic and copies ran while one was open for 9% -> 0% of each run, Pallas kernels for 0% -> 0%
where the time goes in v1:
time: 89.8 us; the launch traced here: 89.5 us
  Pallas kernels  82.2 us (92%)
  local copies, waits for them, and re-layouts  6.47 us (7%)
    pallas_call x1, Pallas kernels, on_device(): pl.pallas_call(functools.partial(exchange_kernel, n_f, n_r), out_shape=(S...  76.4 us
    unnamed x26, local copies, waits for them, and re-layouts  6.47 us
    pallas_call x1, Pallas kernels, on_device(): pl.pallas_call(functools.partial(finish_kernel, d * width * n_t), grid=(s...  5.8 us

profile of v1, /device:TPU:0, one launch (start us, length us, event | category | flops | bytes accessed | tf_op | source)
XLA Modules:
  0.0 89.5 jit_solution(1238311482765983328)
XLA Ops:
  0.6 0.0 copy-start.9
  0.7 0.0 copy-start.8
  0.7 0.0 copy-start.7
  0.7 0.0 copy-start.6
  0.7 0.0 copy-start.5
  0.7 0.0 copy-start.4
  0.7 0.0 copy-start.2
  0.7 0.0 copy-start.1
  0.7 76.4 %exchange.1 = (bf16[2048,1024]{1,0:T(8,128)(2,1)}, bf16[2048,512]{1,0:T(8,128)(2,1)}, bf16[4,2,256,128]{3,2,1,0:T(8,128)(2,1)}, bf16[4,2,64,128]{3,2,1,0:T(8,128)(2,1)}, f32[2,2,8,128]{3,2,1,0:T(8,128)}) custom-call(bf16[1024,2048]{1,0:T(8,128)(2,1)} %x_hbm.1, bf16[1024,512]{1,0:T(8,128)(2,1)} %ci_hbm.1, bf16[1024,512]{1,0:T(8,128)(2,1)} %cg_hbm.1, ...), custom_call_target="tpu_custom_call" | custom-call | tf_op jit(solution)/shard_map/exchange/pallas_call | solution.py:275
  77.2 0.0 copy-done.9
  77.2 0.0 copy-done.8
  77.2 0.0 copy-done.7
  77.2 0.0 copy-done.6
  77.2 0.0 copy-done.5
  77.2 0.0 copy-done.4
  77.2 0.0 copy-done.2
  77.2 0.0 copy-done.1
  77.3 0.0 copy-start
  77.3 2.2 %copy-done = bf16[2048,1024]{1,0:T(8,128)(2,1)S(1)} copy-done((bf16[2048,1024]{1,0:T(8,128)(2,1)S(1)}, bf16[2048,1024]{1,0:T(8,128)(2,1)}, u32[]{:S(2)}) %copy-start) | copy-done | bytes 4194328
  79.4 0.0 copy-start.3
  79.4 1.6 %copy-done.3 = bf16[2048,512]{1,0:T(8,128)(2,1)S(1)} copy-done((bf16[2048,512]{1,0:T(8,128)(2,1)S(1)}, bf16[2048,512]{1,0:T(8,128)(2,1)}, u32[]{:S(2)}) %copy-start.3) | copy-done | bytes 2097176
  81.0 0.0 copy-start.10
  81.0 1.0 %copy-done.10 = bf16[4,2,256,128]{3,2,1,0:T(8,128)(2,1)S(1)} copy-done((bf16[4,2,256,128]{3,2,1,0:T(8,128)(2,1)S(1)}, bf16[4,2,256,128]{3,2,1,0:T(8,128)(2,1)}, u32[]{:S(2)}) %copy-start.10) | copy-done | bytes 524312
  82.1 0.0 copy-start.11
  82.1 0.9 %copy-done.11 = bf16[4,2,64,128]{3,2,1,0:T(8,128)(2,1)S(1)} copy-done((bf16[4,2,64,128]{3,2,1,0:T(8,128)(2,1)S(1)}, bf16[4,2,64,128]{3,2,1,0:T(8,128)(2,1)}, u32[]{:S(2)}) %copy-start.11) | copy-done | bytes 131096
  83.0 0.0 copy-start.12
  83.0 0.7 copy-done.12
  83.7 5.8 %finish.1 = (f32[512,512]{1,0:T(8,128)}, f32[512,512]{1,0:T(8,128)}, f32[512,512]{1,0:T(8,128)}, f32[512,512]{1,0:T(8,128)}, f32[64,512]{1,0:T(8,128)}, /*index=...) custom-call(bf16[2048,512]{1,0:T(8,128)(2,1)S(1)} %copy-done.3, ...), custom_call_target="tpu_custom_call" | custom-call | tf_op jit(solution)/shard_map/finish/pallas_call | solution.py:329
Async XLA Ops:
  0.6 76.5 %copy-start.9 = (f32[64,512]{1,0:T(8,128)S(1)}, f32[64,512]{1,0:T(8,128)}, u32[]{:S(2)}) copy-start(f32[64,512]{1,0:T(8,128)} %s1_.1) | copy-start | bytes 393220
  0.7 76.5 %copy-start.8 = (f32[64,512]{1,0:T(8,128)S(1)}, f32[64,512]{1,0:T(8,128)}, u32[]{:S(2)}) copy-start(f32[64,512]{1,0:T(8,128)} %p1.1) | copy-start | bytes 393220
  0.7 76.5 %copy-start.7 = (f32[64,512]{1,0:T(8,128)S(1)}, f32[64,512]{1,0:T(8,128)}, u32[]{:S(2)}) copy-start(f32[64,512]{1,0:T(8,128)} %s0.1) | copy-start | bytes 393220
  0.7 76.5 %copy-start.6 = (f32[64,512]{1,0:T(8,128)S(1)}, f32[64,512]{1,0:T(8,128)}, u32[]{:S(2)}) copy-start(f32[64,512]{1,0:T(8,128)} %p0.1) | copy-start | bytes 393220
  0.7 76.5 %copy-start.5 = (bf16[512,256]{1,0:T(8,128)(2,1)S(1)}, bf16[512,256]{1,0:T(8,128)(2,1)}, u32[]{:S(2)}) copy-start(bf16[512,256]{1,0:T(8,128)(2,1)} %fg.1) | copy-start | bytes 786436
  0.7 76.5 %copy-start.4 = (bf16[512,256]{1,0:T(8,128)(2,1)S(1)}, bf16[512,256]{1,0:T(8,128)(2,1)}, u32[]{:S(2)}) copy-start(bf16[512,256]{1,0:T(8,128)(2,1)} %fi.1) | copy-start | bytes 786436
  0.7 76.5 %copy-start.2 = (f32[512,512]{1,0:T(8,128)S(1)}, f32[512,512]{1,0:T(8,128)}, u32[]{:S(2)}) copy-start(f32[512,512]{1,0:T(8,128)} %mg.1) | copy-start | bytes 3145732
  0.7 76.5 %copy-start.1 = (f32[512,512]{1,0:T(8,128)S(1)}, f32[512,512]{1,0:T(8,128)}, u32[]{:S(2)}) copy-start(f32[512,512]{1,0:T(8,128)} %mi.1) | copy-start | bytes 3145732
  77.3 2.2 %copy-start = (bf16[2048,1024]{1,0:T(8,128)(2,1)S(1)}, bf16[2048,1024]{1,0:T(8,128)(2,1)}, u32[]{:S(2)}) copy-start(bf16[2048,1024]{1,0:T(8,128)(2,1)} %get-tuple-element.16.mas) | copy-start | bytes 12582916
  79.4 1.6 %copy-start.3 = (bf16[2048,512]{1,0:T(8,128)(2,1)S(1)}, bf16[2048,512]{1,0:T(8,128)(2,1)}, u32[]{:S(2)}) copy-start(bf16[2048,512]{1,0:T(8,128)(2,1)} %get-tuple-element.15.fac) | copy-start | bytes 6291460
  81.0 1.0 %copy-start.10 = (bf16[4,2,256,128]{3,2,1,0:T(8,128)(2,1)S(1)}, bf16[4,2,256,128]{3,2,1,0:T(8,128)(2,1)}, u32[]{:S(2)}) copy-start(bf16[4,2,256,128]{3,2,1,0:T(8,128)(2,1)} %get-tuple-element.17.nor) | copy-start | bytes 1572868
  82.1 0.9 %copy-start.11 = (bf16[4,2,64,128]{3,2,1,0:T(8,128)(2,1)S(1)}, bf16[4,2,64,128]{3,2,1,0:T(8,128)(2,1)}, u32[]{:S(2)}) copy-start(bf16[4,2,64,128]{3,2,1,0:T(8,128)(2,1)} %get-tuple-element.18.low) | copy-start | bytes 393220
  83.0 0.7 copy-start.12

commit v2 on v1

--- a/solution.py
+++ b/solution.py
@@ -131,6 +131,35 @@
             f2[k, j].wait_recv()
         at = span(f_from(k) * rows + t * half, half, half)
         f3[k] = send(fac.at[at], fac.at[at], f3s.at[k], f3r.at[k], f, r, 1 - t)
+    relay = n_r == 4
+    near = [1, 2] if relay else js
+    m2 = {}
+
+    def pair(j):
+        return lax.bitwise_xor(r, j) if relay else r_to(j)
+
+    def spread_masters(k):
+        m1[k].wait_recv()
+        at = span(f_from(k) * rows + r * quarter, quarter, quarter)
+        for j in near:
+            m2[k, j] = send(masters_out.at[at], masters_out.at[at], m2s.at[k, j], m2r.at[k, j], f, pair(j), t)
+
+    def relay_masters(k):
+        for j in near:
+            m2[k, j].wait_recv()
+        if relay:
+            part = quarter // 2
+            for i, j in enumerate(near):
+                start = f_from(k) * rows + pair(j) * quarter + i * part
+                at = span(start, part, part)
+                to = near[1 - i]
+                slot = 0 if i == 0 else 3
+                m2[k, slot] = send(masters_out.at[at], masters_out.at[at], m2s.at[k, slot], m2r.at[k, slot], f, pair(to), t)
+
+    cut1 = (len(ks) + 2) // 3
+    cut2 = (2 * len(ks) + 2) // 3
+    for k in ks[:cut1]:
+        spread_masters(k)
     for k in ks:
         f3[k].wait_recv()
         project(f_from(k), False)
@@ -149,17 +178,9 @@
         for j in js:
             r1[j, g] = send(pbuf.at[r_to(j), g], r1buf.at[j, g], r1s.at[j, g], r1r.at[j, g], f, r_to(j), t)
 
-    m2 = {}
-
-    def spread_masters(k):
-        m1[k].wait_recv()
-        at = span(f_from(k) * rows + r * quarter, quarter, quarter)
-        for j in js:
-            m2[k, j] = send(masters_out.at[at], masters_out.at[at], m2s.at[k, j], m2r.at[k, j], f, r_to(j), t)
-
-    cut1 = (len(ks) + 2) // 3
-    cut2 = (2 * len(ks) + 2) // 3
     for k in ks[:cut1]:
+        relay_masters(k)
+    for k in ks[cut1:cut2]:
         spread_masters(k)
 
     for g in range(2):
@@ -193,6 +214,8 @@
     for j in js:
         al[j] = send(lall.at[r], lall.at[r], als.at[j], alr.at[j], f, r_to(j), t)
     for k in ks[cut1:cut2]:
+        relay_masters(k)
+    for k in ks[cut2:]:
         spread_masters(k)
     for k in ks:
         a1[k].wait_recv()
@@ -200,7 +223,7 @@
     for j in js:
         a2[j] = send(nall.at[r], nall.at[r], a2s.at[j], a2r.at[j], f, r_to(j), t)
     for k in ks[cut2:]:
-        spread_masters(k)
+        relay_masters(k)
     for j in js:
         al[j].wait_recv()
     llow = local(lall, low_out, 13)
@@ -227,7 +250,7 @@
     for c in (lown, lfac, llow, lnorm, lsq):
         c.wait()
     for k in ks:
-        for j in js:
+        for j in ((0, 3) if relay else ()):
             m2[k, j].wait_recv()
     for c in sent:
         c.wait_send()
@@ -338,7 +361,7 @@
         ],
         out_specs=(tiled(rt, width),) * 4 + (moment,) * 4 + (tiled(dt, width),) * 2,
         compiler_params=pltpu.CompilerParams(
-            dimension_semantics=("arbitrary",), vmem_limit_bytes=LIMIT // 2),
+            dimension_semantics=("arbitrary",), vmem_limit_bytes=LIMIT),
         name="finish",
     )(factors, masters, normed, low, squares, fi, fg, mi, mg, p0, s0, p1, s1)
 

time: 89.8 us -> 79.1 us (0.88)
  local copies, waits for them, and re-layouts: 6.47 us -> 0 us
  Pallas kernels: 82.2 us -> 77.6 us
    pallas_call x1, Pallas kernels: 76.4 us -> 66.9 us  [on_device(): pl.pallas_call(functools.partial(exchange_kernel, n_f, n_r), out_shape=(S...]
    unnamed x26 -> x0, local copies, waits for them, and re-layouts: 6.47 us -> none
    pallas_call x1, Pallas kernels: 5.8 us -> 10.7 us  [on_device(): pl.pallas_call(functools.partial(finish_kernel, d * width * n_t), grid=(s...]
where the time goes in v2:
time: 79.1 us; the launch traced here: 78.3 us
  Pallas kernels  77.6 us (98%)
    pallas_call x1, Pallas kernels, on_device(): pl.pallas_call(functools.partial(exchange_kernel, n_f, n_r), out_shape=(S...  66.9 us
    pallas_call x1, Pallas kernels, on_device(): pl.pallas_call(functools.partial(finish_kernel, d * width * n_t), grid=(s...  10.7 us

profile of v2, /device:TPU:0, one launch (start us, length us, event | category | flops | bytes accessed | tf_op | source)
XLA Modules:
  0.0 78.3 jit_solution(3349001819591629875)
XLA Ops:
  0.6 66.9 %exchange.1 = (bf16[2048,1024]{1,0:T(8,128)(2,1)}, bf16[2048,512]{1,0:T(8,128)(2,1)}, bf16[4,2,256,128]{3,2,1,0:T(8,128)(2,1)}, bf16[4,2,64,128]{3,2,1,0:T(8,128)(2,1)}, f32[2,2,8,128]{3,2,1,0:T(8,128)}) custom-call(bf16[1024,2048]{1,0:T(8,128)(2,1)} %x_hbm.1, bf16[1024,512]{1,0:T(8,128)(2,1)} %ci_hbm.1, bf16[1024,512]{1,0:T(8,128)(2,1)} %cg_hbm.1, ...), custom_call_target="tpu_custom_call" | custom-call | tf_op jit(solution)/shard_map/exchange/pallas_call | solution.py:298
  67.5 10.7 %finish.1 = (f32[512,512]{1,0:T(8,128)}, f32[512,512]{1,0:T(8,128)}, f32[512,512]{1,0:T(8,128)}, f32[512,512]{1,0:T(8,128)}, f32[64,512]{1,0:T(8,128)}, /*index=...) custom-call(bf16[2048,512]{1,0:T(8,128)(2,1)} %get-tuple-element.15., ...), custom_call_target="tpu_custom_call" | custom-call | tf_op jit(solution)/shard_map/finish/pallas_call | solution.py:352

commit v3 on v2

--- a/solution.py
+++ b/solution.py
@@ -46,6 +46,13 @@
     def span(start, size, unit):
         return pl.ds(pl.multiple_of(start, unit), size)
 
+    relay = n_r == 4
+    near = [1, 2] if relay else js
+    short = relay and piece % 16 == 0
+
+    def pair(j):
+        return lax.bitwise_xor(r, j) if relay else r_to(j)
+
     sent = []
 
     def send(src, dst, ss, rs, ff, rr, tt):
@@ -72,9 +79,10 @@
     for k in ks:
         pl.semaphore_signal(barrier, inc=1, device_id=(f_to(k), r, t), device_id_type=MESH)
     for j in js:
-        pl.semaphore_signal(barrier, inc=1, device_id=(f, r_to(j), t), device_id_type=MESH)
+        for tt in (t, 1 - t):
+            pl.semaphore_signal(barrier, inc=1, device_id=(f, r_to(j), tt), device_id_type=MESH)
     pl.semaphore_signal(barrier, inc=1, device_id=(f, r, 1 - t), device_id_type=MESH)
-    pl.semaphore_wait(barrier, len(ks) + len(js) + 1)
+    pl.semaphore_wait(barrier, len(ks) + 2 * len(js) + 1)
 
     for c in lf:
         c.wait()
@@ -118,25 +126,30 @@
     def spread(k):
         f1[k].wait_recv()
         at = span(f_from(k) * rows + t * half + r * piece, piece, piece)
-        for j in js:
-            f2[k, j] = send(fac.at[at], fac.at[at], f2s.at[k, j], f2r.at[k, j], f, r_to(j), t)
+        for j in (near if short else js):
+            to = pair(j) if short else r_to(j)
+            f2[k, j] = send(fac.at[at], fac.at[at], f2s.at[k, j], f2r.at[k, j], f, to, t)
 
     if blocked:
         project(f, True)
     for k in ks:
         spread(k)
     f3 = {}
-    for k in ks:
-        for j in js:
+    if short:
+        for k in ks:
+            part = piece // 2
+            for j in near:
+                f2[k, j].wait_recv()
+            for i, j in enumerate(near):
+                at = span(f_from(k) * rows + t * half + pair(j) * piece + i * part, part, part)
+                slot = 3 * i
+                f2[k, slot] = send(fac.at[at], fac.at[at], f2s.at[k, slot], f2r.at[k, slot], f, pair(near[1 - i]), t)
+    for k in ks:
+        for j in ((0, 3) if short else js):
             f2[k, j].wait_recv()
         at = span(f_from(k) * rows + t * half, half, half)
         f3[k] = send(fac.at[at], fac.at[at], f3s.at[k], f3r.at[k], f, r, 1 - t)
-    relay = n_r == 4
-    near = [1, 2] if relay else js
     m2 = {}
-
-    def pair(j):
-        return lax.bitwise_xor(r, j) if relay else r_to(j)
 
     def spread_masters(k):
         m1[k].wait_recv()
@@ -220,33 +233,41 @@
     for k in ks:
         a1[k].wait_recv()
     a2 = {}
-    for j in js:
-        a2[j] = send(nall.at[r], nall.at[r], a2s.at[j], a2r.at[j], f, r_to(j), t)
+    for j in near:
+        a2[j] = send(nall.at[r], nall.at[r], a2s.at[j], a2r.at[j], f, pair(j), t)
+    for g in range(2):
+        quarter_g = nall[r, g]
+
+        def square(i, total):
+            at = span(i * 256, 256, 256)
+            full = jnp.dot(fac[at, g * rank:(g + 1) * rank], quarter_g, preferred_element_type=F32)
+            return total + jnp.sum((full * full).reshape(32, 8, cw), axis=0)
+
+        sq[t, r, g] = lax.fori_loop(0, fac.shape[0] // 256, square, jnp.zeros((8, cw), F32))
+    mysq = sq.at[t, r]
+    qs = {}
+    for j in range(n_r):
+        for i, tt in enumerate((t, 1 - t)):
+            if j or i:
+                qs[j, i] = send(mysq, mysq, sqs.at[j, i], sqr.at[j, i], f, r_to(j), tt)
+    if relay:
+        for j in near:
+            a2[j].wait_recv()
+        for i, j in enumerate(near):
+            at = nall.at[pair(j), i]
+            slot = 3 * i
+            a2[slot] = send(at, at, a2s.at[slot], a2r.at[slot], f, pair(near[1 - i]), t)
     for k in ks[cut2:]:
         relay_masters(k)
     for j in js:
         al[j].wait_recv()
     llow = local(lall, low_out, 13)
-    for j in js:
+    for c in qs.values():
+        c.wait_recv()
+    lsq = local(sq, square_out, 15)
+    for j in ((0, 3) if relay else js):
         a2[j].wait_recv()
     lnorm = local(nall, normed_out, 14)
-
-    for g in range(2):
-        whole = jnp.concatenate([nall[q, g] for q in range(n_r)], axis=1)
-
-        def square(i, total):
-            at = span(i * 256, 256, 256)
-            full = jnp.dot(fac[at, g * rank:(g + 1) * rank], whole, preferred_element_type=F32)
-            return total + jnp.sum((full * full).reshape(32, 8, width), axis=0)
-
-        total = lax.fori_loop(0, fac.shape[0] // 256, square, jnp.zeros((8, width), F32))
-        part = total[:, :128]
-        for q in range(1, width // 128):
-            part = part + total[:, q * 128:(q + 1) * 128]
-        sq[t, g] = part
-    other = send(sq.at[t], sq.at[t], sqs, sqr, f, r, 1 - t)
-    other.wait_recv()
-    lsq = local(sq, square_out, 15)
     for c in (lown, lfac, llow, lnorm, lsq):
         c.wait()
     for k in ks:
@@ -275,7 +296,8 @@
 
     for g, (own_f, own_m, m_new, up, copy) in enumerate(((fi, mi, mi_new, ui, ci), (fg, mg, mg_new, ug, cg))):
         whole = jnp.concatenate([nor[q, g] for q in range(n_r)], axis=1)
-        square = jnp.sum(sqr[0, g] + sqr[1, g], keepdims=True)
+        parts = sum(sqr[i, q, g] for i in range(2) for q in range(n_r))
+        square = jnp.sum(parts, keepdims=True)
         scale = 1.0 / jnp.sqrt(square / entries + 0.1)
         full = jnp.dot(own_f[...], whole, preferred_element_type=F32)
         update = full * scale
@@ -302,7 +324,7 @@
             S((d, 2 * rank), BF),
             S((n_r, 2, rank, cw), BF),
             S((n_r, 2, own, cw), BF),
-            S((2, 2, 8, 128), F32),
+            S((2, n_r, 2, 8, cw), F32),
         ),
         in_specs=[any_] * 11,
         out_specs=(any_,) * 5,
@@ -320,7 +342,7 @@
             pltpu.VMEM((n_f, 2, own, cw), BF),
             pltpu.VMEM((n_r, 2, rank, cw), BF),
             pltpu.VMEM((n_r, 2, own, cw), BF),
-            pltpu.VMEM((2, 2, 8, 128), F32),
+            pltpu.VMEM((2, n_r, 2, 8, cw), F32),
             dma((16,)),
             dma((n_f,)), dma((n_f,)),
             dma((n_f, n_r)), dma((n_f, n_r)),
@@ -332,7 +354,7 @@
             dma((n_f,)), dma((n_f,)),
             dma((n_r,)), dma((n_r,)),
             dma((n_r,)), dma((n_r,)),
-            dma, dma,
+            dma((n_r, 2)), dma((n_r, 2)),
         ],
         compiler_params=pltpu.CompilerParams(
             collective_id=0, has_side_effects=True, vmem_limit_bytes=LIMIT),

time: 79.1 us -> 80 us (1.011)
  the two profiles are of different devices: /device:TPU:0 before, /device:TPU:16 now
where the time goes in v3:
time: 80 us; the launch traced here: 79.7 us
  Pallas kernels  79 us (99%)
    pallas_call x1, Pallas kernels, on_device(): pl.pallas_call(functools.partial(exchange_kernel, n_f, n_r), out_shape=(S...  68.3 us
    pallas_call x1, Pallas kernels, on_device(): pl.pallas_call(functools.partial(finish_kernel, d * width * n_t), grid=(s...  10.8 us

profile of v3, /device:TPU:16, one launch (start us, length us, event | category | flops | bytes accessed | tf_op | source)
XLA Modules:
  0.0 79.7 jit_solution(13205111689677539789)
XLA Ops:
  0.6 68.3 %exchange.1 = (bf16[2048,1024]{1,0:T(8,128)(2,1)}, bf16[2048,512]{1,0:T(8,128)(2,1)}, bf16[4,2,256,128]{3,2,1,0:T(8,128)(2,1)}, bf16[4,2,64,128]{3,2,1,0:T(8,128)(2,1)}, f32[2,4,2,8,128]{4,3,2,1,0:T(8,128)}) custom-call(bf16[1024,2048]{1,0:T(8,128)(2,1)} %x_hbm.1, bf16[1024,512]{1,0:T(8,128)(2,1)} %ci_hbm.1, bf16[1024,512]{1,0:T(8,128)(2,1)} %cg_hbm.1, ...), custom_call_target="tpu_custom_call" | custom-call | tf_op jit(solution)/shard_map/exchange/pallas_call | solution.py:320
  68.9 10.8 %finish.1 = (f32[512,512]{1,0:T(8,128)}, f32[512,512]{1,0:T(8,128)}, f32[512,512]{1,0:T(8,128)}, f32[512,512]{1,0:T(8,128)}, f32[64,512]{1,0:T(8,128)}, /*index=...) custom-call(bf16[2048,512]{1,0:T(8,128)(2,1)} %get-tuple-element.15., ...), custom_call_target="tpu_custom_call" | custom-call | tf_op jit(solution)/shard_map/finish/pallas_call | solution.py:374

commit v4 on v3

--- a/solution.py
+++ b/solution.py
@@ -317,6 +317,7 @@
     any_ = pl.BlockSpec(memory_space=pl.ANY)
     dma = pltpu.SemaphoreType.DMA
     S = jax.ShapeDtypeStruct
+    hx, hci, hcg, hmi, hmg, hfi, hfg, h0, h1, h2, h3 = (pltpu.with_memory_space_constraint(v, pltpu.HBM) for v in (x, ci, cg, mi, mg, fi, fg, p0, s0, p1, s1))
     masters, factors, normed, low, squares = pl.pallas_call(
         functools.partial(exchange_kernel, n_f, n_r),
         out_shape=(
@@ -357,9 +358,9 @@
             dma((n_r, 2)), dma((n_r, 2)),
         ],
         compiler_params=pltpu.CompilerParams(
-            collective_id=0, has_side_effects=True, vmem_limit_bytes=LIMIT),
+            collective_id=0, has_side_effects=True, vmem_limit_bytes=26*1024*1024),
         name="exchange",
-    )(x, ci, cg, mi, mg, fi, fg, p0, s0, p1, s1)
+    )(hx, hci, hcg, hmi, hmg, hfi, hfg, h0, h1, h2, h3)
 
     steps = 8
     dt, rt = d // steps, rows // steps
@@ -383,7 +384,7 @@
         ],
         out_specs=(tiled(rt, width),) * 4 + (moment,) * 4 + (tiled(dt, width),) * 2,
         compiler_params=pltpu.CompilerParams(
-            dimension_semantics=("arbitrary",), vmem_limit_bytes=LIMIT),
+            dimension_semantics=("arbitrary",), vmem_limit_bytes=26*1024*1024),
         name="finish",
     )(factors, masters, normed, low, squares, fi, fg, mi, mg, p0, s0, p1, s1)
 

time: 80 us -> 74.3 us (0.929)
  Pallas kernels: 79 us -> 73.3 us
    pallas_call x1, Pallas kernels: 10.8 us -> 5.88 us  [on_device(): pl.pallas_call(functools.partial(finish_kernel, d * width * n_t), grid=(s...]
where the time goes in v4:
time: 74.3 us; the launch traced here: 74.2 us
  Pallas kernels  73.3 us (99%)
  between operations  0.78 us (1%)
    pallas_call x1, Pallas kernels, on_device(): pl.pallas_call(functools.partial(exchange_kernel, n_f, n_r), out_shape=(S...  67.5 us
    pallas_call x1, Pallas kernels, on_device(): pl.pallas_call(functools.partial(finish_kernel, d * width * n_t), grid=(s...  5.88 us

profile of v4, /device:TPU:16, one launch (start us, length us, event | category | flops | bytes accessed | tf_op | source)
XLA Modules:
  0.0 74.2 jit_solution(10727585122056370766)
XLA Ops:
  0.6 0.0 copy-start.7
  0.7 0.0 copy-start.6
  0.7 0.0 copy-start.5
  0.7 0.0 copy-start.4
  0.7 0.0 copy-start.3
  0.7 0.0 copy-start.2
  0.7 0.0 copy-start.1
  0.7 0.0 copy-start
  0.7 67.5 %exchange.1 = (bf16[2048,1024]{1,0:T(8,128)(2,1)S(1)}, bf16[2048,512]{1,0:T(8,128)(2,1)S(1)}, bf16[4,2,256,128]{3,2,1,0:T(8,128)(2,1)S(1)}, bf16[4,2,64,128]{3,2,1,0:T(8,128)(2,1)S(1)}, f32[2,4,2,8,128]{4,3,2,1,0:T(8,128)S(1)}) custom-call(bf16[1024,2048]{1,0:T(8,128)(2,1)} %x_hbm.1, bf16[1024,512]{1,0:T(8,128)(2,1)} %ci_hbm.1, bf16[1024,512]{1,0:T(8,128)(2,1)} %cg_hbm.1, ...), custom_call_target="tpu_custom_call" | custom-call | tf_op jit(solution)/shard_map/exchange/pallas_call | solution.py:321
  68.2 0.0 copy-done.7
  68.2 0.0 copy-done.6
  68.2 0.0 copy-done.5
  68.2 0.0 copy-done.4
  68.2 0.0 copy-done.3
  68.2 0.0 copy-done.2
  68.3 0.0 copy-done.1
  68.3 0.0 copy-done
  68.3 5.9 %finish.1 = (f32[512,512]{1,0:T(8,128)}, f32[512,512]{1,0:T(8,128)}, f32[512,512]{1,0:T(8,128)}, f32[512,512]{1,0:T(8,128)}, f32[64,512]{1,0:T(8,128)}, /*index=...) custom-call(bf16[2048,512]{1,0:T(8,128)(2,1)S(1)} %get-tuple-element, ...), custom_call_target="tpu_custom_call" | custom-call | tf_op jit(solution)/shard_map/finish/pallas_call | solution.py:375
Async XLA Ops:
  0.6 67.6 %copy-start.7 = (f32[64,512]{1,0:T(8,128)S(1)}, f32[64,512]{1,0:T(8,128)}, u32[]{:S(2)}) copy-start(f32[64,512]{1,0:T(8,128)} %s1_.1) | copy-start | bytes 393220
  0.7 67.6 %copy-start.6 = (f32[64,512]{1,0:T(8,128)S(1)}, f32[64,512]{1,0:T(8,128)}, u32[]{:S(2)}) copy-start(f32[64,512]{1,0:T(8,128)} %p1.1) | copy-start | bytes 393220
  0.7 67.6 %copy-start.5 = (f32[64,512]{1,0:T(8,128)S(1)}, f32[64,512]{1,0:T(8,128)}, u32[]{:S(2)}) copy-start(f32[64,512]{1,0:T(8,128)} %s0.1) | copy-start | bytes 393220
  0.7 67.6 %copy-start.4 = (f32[64,512]{1,0:T(8,128)S(1)}, f32[64,512]{1,0:T(8,128)}, u32[]{:S(2)}) copy-start(f32[64,512]{1,0:T(8,128)} %p0.1) | copy-start | bytes 393220
  0.7 67.6 %copy-start.3 = (bf16[512,256]{1,0:T(8,128)(2,1)S(1)}, bf16[512,256]{1,0:T(8,128)(2,1)}, u32[]{:S(2)}) copy-start(bf16[512,256]{1,0:T(8,128)(2,1)} %fg.1) | copy-start | bytes 786436
  0.7 67.6 %copy-start.2 = (bf16[512,256]{1,0:T(8,128)(2,1)S(1)}, bf16[512,256]{1,0:T(8,128)(2,1)}, u32[]{:S(2)}) copy-start(bf16[512,256]{1,0:T(8,128)(2,1)} %fi.1) | copy-start | bytes 786436
  0.7 67.6 %copy-start.1 = (f32[512,512]{1,0:T(8,128)S(1)}, f32[512,512]{1,0:T(8,128)}, u32[]{:S(2)}) copy-start(f32[512,512]{1,0:T(8,128)} %mg.1) | copy-start | bytes 3145732
  0.7 67.6 %copy-start = (f32[512,512]{1,0:T(8,128)S(1)}, f32[512,512]{1,0:T(8,128)}, u32[]{:S(2)}) copy-start(f32[512,512]{1,0:T(8,128)} %mi.1) | copy-start | bytes 3145732
